TPU v7x, 256 devices: a whole 4x4x8 slice. The times are simulated.
256 devices in a mesh: sp: 16 (over y, x), tp: 16 (over z, core).
Axes of the slice: x: 4, y: 4, z: 8, core: 2. Of those that a mesh axis runs over, the one named last changes fastest.
Arguments:
- residual: bfloat16 [8192, 2048], P(('sp', 'tp')), may hold values from -6 to 6
- queries: bfloat16 [8192, 4096], P('sp', 'tp'), may hold values from -6 to 6
- keys: bfloat16 [8192, 4096], P('sp', 'tp'), may hold values from -6 to 6
- values: bfloat16 [8192, 4096], P('sp', 'tp'), may hold values from -6 to 6
- in_gate: float32 [16, 8192], P('tp', 'sp'), may hold values from -5 to 130
- forget_gate: float32 [16, 8192], P('tp', 'sp'), may hold values from 0 to 16
- doc_ids: int32 [8192], P('sp'), may hold values from 0 to 7, never falling along the last dimension, each value on 1 to 4096 neighbouring positions
- head_gain: float32 [4096], P('tp'), may hold values from 0.1 to 1.9
- out_weight: bfloat16 [4096, 2048], P('tp'), may hold values from -0.09375 to 0.09375
- norm_gain: float32 [2048], replicated, may hold values from 0.1 to 1.9
- route_ids: int32 [8192, 2], P(('sp', 'tp')), may hold values from 0 to 15, all different within a row; in each aligned block of 32 rows (0 to 31, 32 to 63, ...) at most 5 rows name the same one
- route_weights: float32 [8192, 2], P(('sp', 'tp')), may hold values from 0.2 to 1
- gate_proj: bfloat16 [16, 2048, 4096], P('sp', None, 'tp'), may hold values from -0.125 to 0.125
- up_proj: bfloat16 [16, 2048, 4096], P('sp', None, 'tp'), may hold values from -0.125 to 0.125
- down_proj: bfloat16 [16, 4096, 2048], P('sp', 'tp'), may hold values from -0.09375 to 0.09375
Outputs:
- mixed: bfloat16 [8192, 2048], P(('sp', 'tp'))
Inputs may be any that keep to these rules, and one draw needn't show every extreme that they name: `route_ids`: each row names 2 different experts. In each aligned block of 32 rows (the rows of one device) no expert is named by more than 5 rows, and in some blocks one expert by exactly 5. `doc_ids`: numbers never fall along the sequence; no document covers more than half of the 8192 positions, and one covers exactly half.
All inputs are finite; a program needn't handle non-finite values.
Results may differ from a plain program's by a relative error of at most 0.018.
Values may be sent and summed in bfloat16 or wider, within the bound.
A program may use at most 64 MiB of HBM per device.

v0:
```python
import math
import jax
import jax.numpy as jnp
from jax import lax
from jax.sharding import Mesh
from jax.sharding import PartitionSpec as P

SP = ("sp_0", "sp_1")
SP_TP = ("sp_0", "sp_1", "tp")
MASKED = -1e30
EPSILON = 1e-06


def neutral_like(value, identity):
    return jax.tree.map(
        lambda a, e: jnp.broadcast_to(jnp.asarray(e, a.dtype), a.shape), value, identity
    )


def carried_in(value, axes, combine, identity):
    before = start = neutral_like(value, identity)
    running = value
    for axis in reversed(axes):
        peers, index = (lax.axis_size(axis), lax.axis_index(axis))
        pieces = jax.tree.map(lambda part: lax.all_gather(part, axis), running)
        inside, running = (start, start)
        for k in range(peers):
            passed = k < index
            running = combine(running, jax.tree.map(lambda part: part[k], pieces))
            inside = jax.tree.map(lambda new, old: jnp.where(passed, new, old), running, inside)
        before = combine(inside, before)
    return before


def block_step(state, pieces):
    memory, normalizer, max_level, carry_doc = state
    q_block, k_block, v_block, in_block, forget_block, doc_block = pieces
    scaling = q_block.shape[1] ** (-0.5)
    cum_forget = jnp.cumsum(forget_block)
    positions = jnp.arange(q_block.shape[0])
    permitted_mask = (positions[:, None] >= positions[None, :]) & (
        doc_block[:, None] == doc_block[None, :]
    )
    log_weights = jnp.where(
        permitted_mask, cum_forget[:, None] - cum_forget[None, :] + in_block[None, :], MASKED
    )
    carried = jnp.where(doc_block == carry_doc, cum_forget + max_level, MASKED)
    row_max = jnp.maximum(carried, jnp.max(log_weights, axis=1))
    scores = jnp.dot(q_block, k_block.T, preferred_element_type=jnp.float32) * scaling
    weighted = scores * jnp.exp(log_weights - row_max[:, None])
    carry_weight = jnp.exp(carried - row_max)
    query_scaled = q_block.astype(jnp.float32) * scaling
    key_full = k_block.astype(jnp.float32)
    value_full = v_block.astype(jnp.float32)
    readout_numerator = jnp.dot(weighted, value_full, precision=lax.Precision.HIGHEST)
    readout_numerator = readout_numerator + carry_weight[:, None] * jnp.dot(
        query_scaled, memory.T, precision=lax.Precision.HIGHEST
    )
    denominator = jnp.sum(weighted, axis=1) + carry_weight * jnp.dot(
        query_scaled, normalizer, precision=lax.Precision.HIGHEST
    )
    last_doc = doc_block[-1]
    forget_total = cum_forget[-1]
    log_end = jnp.where(doc_block == last_doc, forget_total - cum_forget + in_block, MASKED)
    carry_log = jnp.where(carry_doc == last_doc, forget_total + max_level, MASKED)
    new_max = jnp.maximum(carry_log, jnp.max(log_end))
    end_weight = jnp.exp(log_end - new_max)
    kept_share = jnp.exp(carry_log - new_max)
    new_memory = kept_share * memory + jnp.dot(
        (value_full * end_weight[:, None]).T, key_full, precision=lax.Precision.HIGHEST
    )
    new_normalizer = kept_share * normalizer + jnp.dot(
        end_weight, key_full, precision=lax.Precision.HIGHEST
    )
    return (
        (new_memory, new_normalizer, new_max, last_doc),
        (readout_numerator, denominator, row_max),
    )


def run_blocks(
    queries_in,
    keys_in,
    incoming_vectors,
    in_gates,
    log_forget,
    doc_row,
    memory,
    normalizer,
    max_level,
    carry_doc,
):
    extent = queries_in.shape[0]
    block_size = math.gcd(extent, 256)
    blocks = extent // block_size

    def to_blocks(tensor):
        return tensor.reshape((blocks, block_size) + tensor.shape[1:])

    pieces = tuple(
        (
            to_blocks(tensor)
            for tensor in (queries_in, keys_in, incoming_vectors, in_gates, log_forget, doc_row)
        )
    )
    final_state, outputs = lax.scan(block_step, (memory, normalizer, max_level, carry_doc), pieces)
    readout_numerator, denominator, row_max = outputs
    return (
        readout_numerator.reshape(extent, -1),
        denominator.reshape(extent),
        row_max.reshape(extent),
        final_state,
    )


def combine_states(earlier, later):
    memory_a, normal_a, level_a, forget_a, first_a, last_a = earlier
    memory_b, normal_b, level_b, forget_b, first_b, last_b = later
    joined = (last_a == first_b) | (last_a < 0) | (first_b < 0)
    passed = forget_b + jnp.where(joined, 0.0, MASKED)
    new_level = jnp.maximum(passed + level_a, level_b)
    share_a = jnp.exp(passed + level_a - new_level)
    fraction_second = jnp.exp(level_b - new_level)
    new_memory = share_a[:, None, None] * memory_a + fraction_second[:, None, None] * memory_b
    new_normal = share_a[:, None] * normal_a + fraction_second[:, None] * normal_b
    first_doc = jnp.where(first_a < 0, first_b, first_a)
    last_doc = jnp.where(last_b < 0, last_a, last_b)
    return (new_memory, new_normal, new_level, forget_a + passed, first_doc, last_doc)


def on_device(
    residual,
    queries,
    keys,
    values,
    in_gate,
    forget_gate,
    doc_ids,
    head_gain,
    out_weight,
    norm_gain,
    route_ids,
    route_weights,
    gate_proj,
    up_proj,
    down_proj,
):
    extent, local_width = queries.shape
    heads_here = in_gate.shape[0]
    head_size = local_width // heads_here

    def by_head(tensor):
        return tensor.reshape(extent, heads_here, head_size).transpose(1, 0, 2)

    query_heads = by_head(queries)
    key_heads = by_head(keys)
    value_heads = by_head(values)
    log_forget = jax.nn.log_sigmoid(forget_gate)
    cum_forget = jnp.cumsum(log_forget, axis=1)
    first_doc = doc_ids[0]
    last_doc = doc_ids[-1]
    run_heads = jax.vmap(run_blocks, in_axes=(0, 0, 0, 0, 0, None, 0, 0, 0, None))
    forget_total = jnp.where(first_doc == last_doc, cum_forget[:, -1], MASKED)
    doc_first = first_doc.astype(jnp.float32).reshape(1)
    doc_last = last_doc.astype(jnp.float32).reshape(1)
    empty_memory = jnp.zeros((heads_here, head_size, head_size), jnp.float32)
    empty_normal = jnp.zeros((heads_here, head_size), jnp.float32)
    empty_level = jnp.full((heads_here,), MASKED, jnp.float32)
    identity = (
        empty_memory,
        empty_normal,
        empty_level,
        jnp.zeros((heads_here,), jnp.float32),
        jnp.full((1,), -1.0, jnp.float32),
        jnp.full((1,), -1.0, jnp.float32),
    )
    readout_numerator, denominator, row_max, final_state = run_heads(
        query_heads,
        key_heads,
        value_heads,
        in_gate,
        log_forget,
        doc_ids,
        empty_memory,
        empty_normal,
        empty_level,
        first_doc,
    )
    local_state = (
        final_state[0],
        final_state[1],
        final_state[2],
        forget_total,
        doc_first,
        doc_last,
    )
    incoming = carried_in(local_state, SP, combine_states, identity)
    linked = incoming[5][0] == doc_first[0]
    in_level = jnp.where(linked, incoming[2], MASKED)
    carried = jnp.where(doc_ids[None, :] == first_doc, cum_forget + in_level[:, None], MASKED)
    new_max = jnp.maximum(row_max, carried)
    own_share = jnp.exp(row_max - new_max)
    far_share = jnp.exp(carried - new_max)
    query_scaled = query_heads.astype(jnp.float32) * head_size ** (-0.5)
    readout_numerator = own_share[..., None] * readout_numerator + far_share[
        ..., None
    ] * jnp.einsum("htd,hvd->htv", query_scaled, incoming[0], precision=lax.Precision.HIGHEST)
    denominator = own_share * denominator + far_share * jnp.einsum(
        "htd,hd->ht", query_scaled, incoming[1], precision=lax.Precision.HIGHEST
    )
    mixed_heads = (
        readout_numerator / jnp.maximum(jnp.abs(denominator), jnp.exp(-new_max))[..., None]
    )
    normed_heads = mixed_heads * lax.rsqrt(
        jnp.mean(mixed_heads * mixed_heads, axis=-1, keepdims=True) + EPSILON
    )
    normed_heads = normed_heads * head_gain.reshape(heads_here, 1, head_size)
    head_rows = normed_heads.transpose(1, 0, 2).reshape(extent, local_width).astype(jnp.bfloat16)
    rows_here, model_width = residual.shape
    update = lax.psum_scatter(
        jnp.dot(head_rows, out_weight, preferred_element_type=jnp.float32).astype(jnp.bfloat16),
        "tp",
        scatter_dimension=0,
        tiled=True,
    ).astype(jnp.float32)
    stream = residual.astype(jnp.float32) + update
    normed = (
        stream * lax.rsqrt(jnp.mean(stream * stream, axis=-1, keepdims=True) + EPSILON) * norm_gain
    )
    normed = normed.astype(jnp.bfloat16)
    experts_all = gate_proj.shape[0] * lax.axis_size(SP)
    top_count = route_ids.shape[1]
    capacity = max(2, rows_here * top_count * 5 // (4 * experts_all))
    flat_ids = route_ids.reshape(-1)
    onehot = (flat_ids[:, None] == jnp.arange(experts_all, dtype=jnp.int32)[None, :]).astype(
        jnp.int32
    )
    earlier = jnp.cumsum(onehot, axis=0) - onehot
    slot_rank = jnp.sum(earlier * onehot, axis=1)
    slot_index = flat_ids * capacity + slot_rank
    placing = (
        slot_index[None, :] == jnp.arange(experts_all * capacity, dtype=jnp.int32)[:, None]
    ).astype(jnp.bfloat16)
    copies = jnp.repeat(normed, top_count, axis=0)
    outgoing = jnp.dot(placing, copies, preferred_element_type=jnp.float32).astype(jnp.bfloat16)
    outgoing = outgoing.reshape(experts_all, capacity, model_width)
    arrived = lax.all_to_all(outgoing, SP, split_axis=0, concat_axis=0, tiled=True).reshape(
        -1, model_width
    )
    piece = lax.all_gather(arrived, "tp", axis=0, tiled=True)
    gate_part = jnp.dot(piece, gate_proj[0], preferred_element_type=jnp.float32)
    up_part = jnp.dot(piece, up_proj[0], preferred_element_type=jnp.float32)
    hidden = (jax.nn.silu(gate_part) * up_part).astype(jnp.bfloat16)
    expert_sum = lax.psum_scatter(
        jnp.dot(hidden, down_proj[0], preferred_element_type=jnp.float32).astype(jnp.bfloat16),
        "tp",
        scatter_dimension=0,
        tiled=True,
    )
    expert_out = expert_sum.reshape(experts_all, capacity, model_width)
    returned = lax.all_to_all(expert_out, SP, split_axis=0, concat_axis=0, tiled=True)
    picked = jnp.take(returned.reshape(-1, model_width), slot_index, axis=0)
    picked = picked.reshape(rows_here, top_count, model_width)
    expert_mix = jnp.sum(route_weights[..., None] * picked.astype(jnp.float32), axis=1)
    return (stream + expert_mix).astype(jnp.bfloat16)


def solution(mesh):
    finer = Mesh(mesh.devices.reshape(4, 4, mesh.shape["tp"]), ("sp_0", "sp_1", "tp"))
    in_specs = (
        P(SP_TP, None),
        P(SP, "tp"),
        P(SP, "tp"),
        P(SP, "tp"),
        P("tp", SP),
        P("tp", SP),
        P(SP),
        P("tp"),
        P("tp", None),
        P(),
        P(SP_TP, None),
        P(SP_TP, None),
        P(SP, None, "tp"),
        P(SP, None, "tp"),
        P(SP, "tp", None),
    )
    out_specs = P(SP_TP, None)
    return jax.shard_map(
        on_device, mesh=finer, in_specs=in_specs, out_specs=out_specs, check_vma=False
    )
```

profile of v0, /device:TPU:2, one launch (start us, length us, event | category | flops | bytes accessed | tf_op | source)
XLA Modules:
  0.0 372.2 jit_solution(4518122679349654062)
XLA Ops:
  6.5 1.4 fusion.182
  10.0 25.1 %while.23 = (s32[]{:T(128)}, f32[1,256,256]{2,1,0:T(8,128)S(1)}, f32[1,256]{1,0:T(1,128)S(1)}, f32[1]{0:T(128)}, s32[]{:T(128)}, /*index=5*/f32[2,1,256,256]{3,2...) while((s32[]{:T(128)}, f32[1,256,256]{2,1,0:T(8,128)S(1)}, ...), condition=%wide.region_6.7_spmd.clone, body=%wide.region_0.6_spmd.clone.sunk | while | flops 641046528 | bytes 6349332 | solution.py:106
  13.2 1.3 fusion.226
  15.7 1.9 fusion.223
  17.6 1.3 fusion.227
  24.5 1.2 fusion.225
  25.7 1.3 fusion.226
  28.2 1.9 fusion.223
  30.1 1.3 fusion.227
  45.2 10.0 %all-reduce.8 = (f32[4]{0:T(128)S(1)}, f32[4]{0:T(128)S(1)}, f32[4]{0:T(128)S(1)}, f32[4]{0:T(128)S(1)}) all-reduce(f32[4]{0:T(128)S(1)} %dynamic-update-slice, f32[4]{0:T(128)S(1)} %fusion.156, f32[4]{0:T(128)S(1)} %dynamic-update-slice.3, f32[4]{0:T(128)S(1)} %dynamic-update-slice.6), channel_id=1, replica_groups=mesh['sp_0'=4,'sp_1'=4,'tp'=16] {'sp_1'}, use_global_device_ids=true, to_apply=%add | all-reduce | flops 16 | bytes 128
  55.9 2.6 fusion.152
  65.8 1.2 fusion.189
  72.3 2.0 fusion.70
  75.1 1.9 fusion.188
  78.2 1.4 dynamic-update-slice.7
  80.3 1.4 dynamic-update-slice.5
  81.8 1.4 dynamic-update-slice.1
  83.2 9.3 %all-reduce.9 = (f32[4]{0:T(128)S(1)}, f32[4]{0:T(128)S(1)}, f32[4]{0:T(128)S(1)}, f32[4]{0:T(128)S(1)}) all-reduce(f32[4]{0:T(128)S(1)} %dynamic-update-slice.1, f32[4]{0:T(128)S(1)} %dynamic-update-slice.4, f32[4]{0:T(128)S(1)} %dynamic-update-slice.5, f32[4]{0:T(128)S(1)} %dynamic-update-slice.7), channel_id=2, replica_groups=mesh['sp_0'=4,'sp_1'=4,'tp'=16] {'sp_0'}, use_global_device_ids=true, to_apply=%add.1 | all-reduce | flops 16 | bytes 128
  121.3 9.6 %all-gather.8 = f32[4,1,256]{2,1,0:T(1,128)S(1)} all-gather(f32[1,1,256]{2,1,0:T(1,128)S(1)} %bitcast.322), channel_id=9, replica_groups=mesh['sp_0'=4,'sp_1'=4,'tp'=16] {'sp_1'}, dimensions={0}, use_global_device_ids=true | all-gather | bytes 5120 | tf_op jit(solution)/shard_map/all_gather | solution.py:25
  130.9 7.0 %all_gather.84 = f32[4,1,256]{2,1,0:T(1,128)S(1)} all-gather(f32[1,1,256]{2,1,0:T(1,128)S(1)} %get-tuple-element.176), channel_id=1, replica_groups=mesh['sp_0'=4,'sp_1'=4,'tp'=16] {'sp_0'}, dimensions={0}, use_global_device_ids=true | all-gather | bytes 5120 | tf_op jit(solution)/shard_map/all_gather | solution.py:25
  139.3 2.6 multiply_reduce_fusion.1
  141.9 2.2 convolution_convert_fusion.1
  144.7 59.9 %reduce-scatter.3.cloned.1.call-done = bf16[32,2048]{1,0:T(8,128)(2,1)} async-done(((bf16[512,2048]{1,0:T(8,128)(2,1)}), bf16[32,2048]{1,0:T(8,128)(2,1)}) %reduce-scatter.3.cloned.1.call-update) | async-done | bytes 131088 | tf_op jit(solution)/shard_map/reduce_scatter | solution.py:220
  207.4 15.9 %all_to_all.10 = bf16[16,5,2048]{2,1,0:T(8,128)(2,1)S(1)} all-to-all(bf16[16,5,2048]{2,1,0:T(8,128)(2,1)S(1)} %reshape.898), channel_id=1, replica_groups=mesh['sp_0'=4,'sp_1'=4,'tp'=16] {'sp_0','sp_1'}, dimensions={0} | all-to-all | bytes 655360 | tf_op jit(solution)/shard_map/all_to_all | solution.py:247
  224.4 40.1 %all-gather.15.cloned.1.call-done = bf16[1280,2048]{1,0:T(8,128)(2,1)} async-done(((bf16[80,2048]{1,0:T(8,128)(2,1)}), bf16[1280,2048]{1,0:T(8,128)(2,1)}) %all-gather.15.cloned.1.call-update) | async-done | bytes 5242896 | tf_op jit(solution)/shard_map/all_gather | solution.py:250
  264.5 5.1 %fusion.56 = f32[1280,256]{1,0:T(8,128)} fusion(bf16[1280,2048]{1,0:T(8,128)(2,1)} %all-gather.15.cloned.1.call-done, bf16[1,2048,256]{2,1,0:T(8,128)(2,1)S(1)} %copy-done.14), kind=kOutput, calls=%fused_computation.85 | convolution fusion | flops 1342177280 | bytes 7602176 | tf_op jit(solution)/shard_map/dot_general | solution.py:251
  269.6 10.6 %convolution_convert_fusion = bf16[1280,2048]{1,0:T(8,128)(2,1)} fusion(bf16[1280,2048]{1,0:T(8,128)(2,1)} %all-gather.15.cloned.1.call-done, f32[1280,256]{1,0:T(8,128)} %fusion.56, bf16[1,256,2048]{2,1,0:T(8,128)(2,1)S(1)} %copy-done, bf16[1,2048,256]{2,1,0:T(8,128)(2,1)S(1)} %copy-done.15), kind=kOutput, calls=%fused_computation.75 | convolution fusion | flops 2688942080 | bytes 13893632 | tf_op jit(solution)/shard_map/dot_general | solution.py:255
  280.9 63.2 %reduce-scatter.5.cloned.1.call-done = bf16[80,2048]{1,0:T(8,128)(2,1)} async-done(((bf16[1280,2048]{1,0:T(8,128)(2,1)}), bf16[80,2048]{1,0:T(8,128)(2,1)}) %reduce-scatter.5.cloned.1.call-update) | async-done | bytes 327696 | tf_op jit(solution)/shard_map/reduce_scatter | solution.py:254
  344.2 1.9 reshape.900
  346.1 7.3 %all-to-all-start.1 = ((bf16[16,5,2048]{2,1,0:T(8,128)(2,1)}), bf16[16,5,2048]{2,1,0:T(8,128)(2,1)S(1)}, u32[]{:S(2)}, u32[]{:S(2)}) async-start(bf16[16,5,2048]{2,1,0:T(8,128)(2,1)} %reshape.900), calls=%async_computation.3 | async-start | bytes 1048576 | tf_op jit(solution)/shard_map/all_to_all | solution.py:261
  353.4 8.7 %all-to-all-done.1 = bf16[16,5,2048]{2,1,0:T(8,128)(2,1)S(1)} async-done(((bf16[16,5,2048]{2,1,0:T(8,128)(2,1)}), bf16[16,5,2048]{2,1,0:T(8,128)(2,1)S(1)}, u32[]{:S(2)}, u32[]{:S(2)}) %all-to-all-start.1) | async-done | bytes 327712 | tf_op jit(solution)/shard_map/all_to_all | solution.py:261
  363.2 1.8 multiply_reduce_fusion
  (161 shorter events, 32.4 us)
Async XLA Ops:
  6.5 263.0 %copy-start = (bf16[1,256,2048]{2,1,0:T(8,128)(2,1)S(1)}, bf16[1,256,2048]{2,1,0:T(8,128)(2,1)}, u32[]{:S(2)}) copy-start(bf16[1,256,2048]{2,1,0:T(8,128)(2,1)} %param.31) | copy-start | bytes 3145732
  6.5 65.7 %all-gather.17.cloned.1.call-start = ((), (), s32[]{:S(2)}) async-start(), calls=%async_computation.8 | async-start | bytes 1310720 | tf_op jit(solution)/shard_map/all_gather | solution.py:25
  10.0 31.6 %copy-start.17 = (u32[256]{0:T(256)S(1)}, u32[256]{0:T(256)}, u32[]{:S(2)}) copy-start(u32[256]{0:T(256)} %constant.127) | copy-start | bytes 3076
  10.0 64.3 %copy-start.16 = (u32[256]{0:T(256)S(1)}, u32[256]{0:T(256)}, u32[]{:S(2)}) copy-start(u32[256]{0:T(256)} %constant.132) | copy-start | bytes 3076
  10.1 10.8 %copy-start.4 = (bf16[2,1,256,256]{3,2,1,0:T(8,128)(2,1)S(1)}, bf16[2,1,256,256]{3,2,1,0:T(8,128)(2,1)}, u32[]{:S(2)}) copy-start(bf16[2,1,256,256]{3,2,1,0:T(8,128)(2,1)} %get-tuple-element.388) | copy-start | bytes 786436 | tf_op jit(solution)/shard_map/vmap()/while
  10.1 10.8 %copy-start.5 = (bf16[2,1,256,256]{3,2,1,0:T(8,128)(2,1)S(1)}, bf16[2,1,256,256]{3,2,1,0:T(8,128)(2,1)}, u32[]{:S(2)}) copy-start(bf16[2,1,256,256]{3,2,1,0:T(8,128)(2,1)} %get-tuple-element.387) | copy-start | bytes 786436 | tf_op jit(solution)/shard_map/vmap()/while
  10.1 11.3 %copy-start.2 = (bf16[2,1,256,256]{3,2,1,0:T(8,128)(2,1)S(1)}, bf16[2,1,256,256]{3,2,1,0:T(8,128)(2,1)}, u32[]{:S(2)}) copy-start(bf16[2,1,256,256]{3,2,1,0:T(8,128)(2,1)} %get-tuple-element.389) | copy-start | bytes 786436 | tf_op jit(solution)/shard_map/vmap()/while
  22.6 10.8 %copy-start.4 = (bf16[2,1,256,256]{3,2,1,0:T(8,128)(2,1)S(1)}, bf16[2,1,256,256]{3,2,1,0:T(8,128)(2,1)}, u32[]{:S(2)}) copy-start(bf16[2,1,256,256]{3,2,1,0:T(8,128)(2,1)} %get-tuple-element.388) | copy-start | bytes 786436 | tf_op jit(solution)/shard_map/vmap()/while
  22.6 10.8 %copy-start.5 = (bf16[2,1,256,256]{3,2,1,0:T(8,128)(2,1)S(1)}, bf16[2,1,256,256]{3,2,1,0:T(8,128)(2,1)}, u32[]{:S(2)}) copy-start(bf16[2,1,256,256]{3,2,1,0:T(8,128)(2,1)} %get-tuple-element.387) | copy-start | bytes 786436 | tf_op jit(solution)/shard_map/vmap()/while
  22.6 11.3 %copy-start.2 = (bf16[2,1,256,256]{3,2,1,0:T(8,128)(2,1)S(1)}, bf16[2,1,256,256]{3,2,1,0:T(8,128)(2,1)}, u32[]{:S(2)}) copy-start(bf16[2,1,256,256]{3,2,1,0:T(8,128)(2,1)} %get-tuple-element.389) | copy-start | bytes 786436 | tf_op jit(solution)/shard_map/vmap()/while
  35.1 0.7 copy-start.1
  35.1 102.7 %copy-start.9 = (s32[512]{0:T(512)S(1)}, s32[512]{0:T(512)}, u32[]{:S(2)}) copy-start(s32[512]{0:T(512)} %param.23) | copy-start | bytes 6148
  35.2 103.5 %copy-start.3 = (bf16[2,1,256,256]{3,2,1,0:T(8,128)(2,1)S(1)}, bf16[2,1,256,256]{3,2,1,0:T(8,128)(2,1)}, u32[]{:S(2)}) copy-start(bf16[2,1,256,256]{3,2,1,0:T(8,128)(2,1)} %get-tuple-element.404) | copy-start | bytes 786436
  35.9 103.4 %all-gather.13.cloned.1.call-start = ((), (), s32[]{:S(2)}) async-start(), calls=%async_computation.4 | async-start | bytes 1310720 | tf_op jit(solution)/shard_map/all_gather | solution.py:25
  74.3 130.3 %reduce-scatter.3.cloned.1.call-start = ((), (), s32[]{:S(2)}) async-start(), calls=%async_computation.5 | async-start | bytes 2228224 | tf_op jit(solution)/shard_map/reduce_scatter | solution.py:220
  139.3 2.6 copy-start.8
  139.3 2.6 copy-start.13
  141.9 2.3 copy-start.10
  141.9 62.7 %copy-start.6 = (bf16[32,2048]{1,0:T(8,128)(2,1)S(1)}, bf16[32,2048]{1,0:T(8,128)(2,1)}, u32[]{:S(2)}) copy-start(bf16[32,2048]{1,0:T(8,128)(2,1)} %param.17) | copy-start | bytes 393220
  144.1 61.6 %copy-start.11 = (f32[2048]{0:T(1024)S(1)}, f32[2048]{0:T(1024)}, u32[]{:S(2)}) copy-start(f32[2048]{0:T(1024)} %param.26) | copy-start | bytes 24580
  144.1 120.3 %all-gather.15.cloned.1.call-start = ((), (), s32[]{:S(2)}) async-start(), calls=%async_computation.6 | async-start | bytes 5570560 | tf_op jit(solution)/shard_map/all_gather | solution.py:250
  206.9 57.6 %copy-start.14 = (bf16[1,2048,256]{2,1,0:T(8,128)(2,1)S(1)}, bf16[1,2048,256]{2,1,0:T(8,128)(2,1)}, u32[]{:S(2)}) copy-start(bf16[1,2048,256]{2,1,0:T(8,128)(2,1)} %param.29) | copy-start | bytes 3145732
  224.1 45.4 %copy-start.15 = (bf16[1,2048,256]{2,1,0:T(8,128)(2,1)S(1)}, bf16[1,2048,256]{2,1,0:T(8,128)(2,1)}, u32[]{:S(2)}) copy-start(bf16[1,2048,256]{2,1,0:T(8,128)(2,1)} %param.30) | copy-start | bytes 3145732
  224.2 120.0 %reduce-scatter.5.cloned.1.call-start = ((), (), s32[]{:S(2)}) async-start(), calls=%async_computation.7 | async-start | bytes 5570560 | tf_op jit(solution)/shard_map/reduce_scatter | solution.py:254
  280.2 0.7 copy-start.12
  346.1 16.1 %all-to-all-start.1 = ((bf16[16,5,2048]{2,1,0:T(8,128)(2,1)}), bf16[16,5,2048]{2,1,0:T(8,128)(2,1)S(1)}, u32[]{:S(2)}, u32[]{:S(2)}) async-start(bf16[16,5,2048]{2,1,0:T(8,128)(2,1)} %reshape.900), calls=%async_computation.3 | async-start | bytes 1048576 | tf_op jit(solution)/shard_map/all_to_all | solution.py:261
  353.4 11.6 %copy-start.7 = (bf16[32,2048]{1,0:T(8,128)(2,1)S(1)}, bf16[32,2048]{1,0:T(8,128)(2,1)}, u32[]{:S(2)}) copy-start(bf16[32,2048]{1,0:T(8,128)(2,1)} %reduce-scatter.3.cloned.1.call-done) | copy-start | bytes 393220
Sparse Core Ops, SparseCore 0:
  36.0 28.4 all-gather.16
  74.5 28.0 all-gather.12
  144.2 60.3 reduce-scatter.2
  224.3 40.1 all-gather.14
  280.3 63.8 reduce-scatter.4
where the time goes:
time: 374 us; the launch traced here: 372 us
  waiting for transfers between devices  172 us (46%)
  between operations  55.8 us (15%)
  blocking collectives  51.8 us (14%)
  matrix products  30.8 us (8%)
  local copies, waits for them, and re-layouts  25.3 us (7%)
  other arithmetic  23.4 us (6%)
  starting transfers between devices  7.62 us (2%)
  loops' own time  5.4 us (1%)
    reduce_scatter x1, waiting for transfers between devices, on_device(): lax.psum_scatter(jnp.dot(hidden, down_proj[0], preferred_element_type=jnp...  63.2 us
    reduce_scatter x1, waiting for transfers between devices, on_device(): lax.psum_scatter(jnp.dot(head_rows, out_weight, preferred_element_type=jn...  59.9 us
    all_gather x1, waiting for transfers between devices, on_device(): piece = lax.all_gather(arrived, 'tp', axis=0, tiled=True)  40.1 us
    unnamed x2, blocking collectives  19.3 us
    all_gather x2, blocking collectives, carried_in(): pieces = jax.tree.map(lambda part: lax.all_gather(part, axis), running)  16.6 us
    all_to_all x1, blocking collectives, on_device(): lax.all_to_all(outgoing, SP, split_axis=0, concat_axis=0, tiled=True)  15.9 us
    dot_general x1, matrix products, on_device(): jnp.dot(hidden, down_proj[0], preferred_element_type=jnp.float32)  10.6 us
    unnamed x49, local copies, waits for them, and re-layouts  9.59 us
  transfers between devices with their start and end apart: 6, of which 4 were waited for; matrix products, arithmetic and copies ran while one was open for 7% of the time, Pallas kernels for 0%

commit v1 on v0

--- a/solution.py
+++ b/solution.py
@@ -9,6 +9,19 @@
 SP_TP = ("sp_0", "sp_1", "tp")
 MASKED = -1e30
 EPSILON = 1e-06
+
+
+def gather_around(x, axis, dim):
+    ways = lax.axis_size(axis)
+    up = [(d, (d + 1) % ways) for d in range(ways)]
+    down = [(d, (d - 1) % ways) for d in range(ways)]
+    earlier, later = ([x], [x])
+    for _ in range(ways // 2):
+        earlier.append(lax.ppermute(earlier[-1], axis, up))
+    for _ in range((ways - 1) // 2):
+        later.append(lax.ppermute(later[-1], axis, down))
+    line = jnp.concatenate([*earlier[::-1], *later[1:]], axis=dim)
+    return jnp.roll(line, (lax.axis_index(axis) - ways // 2) * x.shape[dim], axis=dim)
 
 
 def neutral_like(value, identity):
@@ -247,7 +260,7 @@
     arrived = lax.all_to_all(outgoing, SP, split_axis=0, concat_axis=0, tiled=True).reshape(
         -1, model_width
     )
-    piece = lax.all_gather(arrived, "tp", axis=0, tiled=True)
+    piece = gather_around(arrived, "tp", 0)
     gate_part = jnp.dot(piece, gate_proj[0], preferred_element_type=jnp.float32)
     up_part = jnp.dot(piece, up_proj[0], preferred_element_type=jnp.float32)
     hidden = (jax.nn.silu(gate_part) * up_part).astype(jnp.bfloat16)

time: 374 us -> 414 us (1.11)
  starting transfers between devices: 7.62 us -> 28.5 us
  local copies, waits for them, and re-layouts: 25.3 us -> 40.8 us
  matrix products: 30.8 us -> 35.2 us
    ppermute x0 -> x15, waiting for transfers between devices: none -> 40.2 us  [the longest x8 38.8 us: gather_around(): earlier.append(lax.ppermute(earlier[-1], axis, up))]
    all_gather x1 -> x0, waiting for transfers between devices: 40.1 us -> none  [on_device(): piece = lax.all_gather(arrived, 'tp', axis=0, tiled=True)]
    ppermute x0 -> x15, starting transfers between devices: none -> 21.1 us  [the longest x7 21.1 us: gather_around(): later.append(lax.ppermute(later[-1], axis, down))]
    unnamed x49 -> x94, local copies, waits for them, and re-layouts: 9.59 us -> 25.9 us
  transfers between devices with their start and end apart: 6 -> 20, of which waited for: 4 -> 13; matrix products, arithmetic and copies ran while one was open for 7% -> 8% of each run, Pallas kernels for 0% -> 0%
where the time goes in v1:
time: 414 us; the launch traced here: 412 us
  waiting for transfers between devices  170 us (41%)
  between operations  56.4 us (14%)
  blocking collectives  51.8 us (13%)
  local copies, waits for them, and re-layouts  40.8 us (10%)
  matrix products  35.2 us (9%)
  starting transfers between devices  28.5 us (7%)
  other arithmetic  23.3 us (6%)
  loops' own time  5.38 us (1%)
    reduce_scatter x1, waiting for transfers between devices, on_device(): lax.psum_scatter(jnp.dot(hidden, down_proj[0], preferred_element_type=jnp...  61.4 us
    reduce_scatter x1, waiting for transfers between devices, on_device(): lax.psum_scatter(jnp.dot(head_rows, out_weight, preferred_element_type=jn...  60 us
    ppermute x8, waiting for transfers between devices, gather_around(): earlier.append(lax.ppermute(earlier[-1], axis, up))  38.8 us
    unnamed x94, local copies, waits for them, and re-layouts  25.9 us
    ppermute x7, starting transfers between devices, gather_around(): later.append(lax.ppermute(later[-1], axis, down))  21.1 us
    unnamed x2, blocking collectives  19.3 us
    all_gather x2, blocking collectives, carried_in(): pieces = jax.tree.map(lambda part: lax.all_gather(part, axis), running)  16.6 us
    all_to_all x1, blocking collectives, on_device(): lax.all_to_all(outgoing, SP, split_axis=0, concat_axis=0, tiled=True)  15.8 us
  transfers between devices with their start and end apart: 20, of which 13 were waited for; matrix products, arithmetic and copies ran while one was open for 8% of the time, Pallas kernels for 0%

profile of v1, /device:TPU:2, one launch (start us, length us, event | category | flops | bytes accessed | tf_op | source)
XLA Modules:
  0.0 411.8 jit_solution(493444347262639)
XLA Ops:
  10.1 30.5 %while.23 = (s32[]{:T(128)}, f32[1,256,256]{2,1,0:T(8,128)S(1)}, f32[1,256]{1,0:T(1,128)S(1)}, f32[1]{0:T(128)}, s32[]{:T(128)}, /*index=5*/f32[2,1,256,256]{3,2...) while((s32[]{:T(128)}, f32[1,256,256]{2,1,0:T(8,128)S(1)}, ...), condition=%wide.region_6.7_spmd.clone, body=%wide.region_0.6_spmd.clone.sunk | while | flops 641046528 | bytes 3205044 | solution.py:119
  50.1 10.0 %all-reduce.8 = (f32[4]{0:T(128)S(1)}, f32[4]{0:T(128)S(1)}, f32[4]{0:T(128)S(1)}, f32[4]{0:T(128)S(1)}) all-reduce(f32[4]{0:T(128)S(1)} %dynamic-update-slice, f32[4]{0:T(128)S(1)} %fusion.165, f32[4]{0:T(128)S(1)} %dynamic-update-slice.3, f32[4]{0:T(128)S(1)} %dynamic-update-slice.6), channel_id=1, replica_groups=mesh['sp_0'=4,'sp_1'=4,'tp'=16] {'sp_1'}, use_global_device_ids=true, to_apply=%add | all-reduce | flops 16 | bytes 128
  60.8 2.6 fusion.161
  77.4 2.0 fusion.79
  87.9 9.3 %all-reduce.9 = (f32[4]{0:T(128)S(1)}, f32[4]{0:T(128)S(1)}, f32[4]{0:T(128)S(1)}, f32[4]{0:T(128)S(1)}) all-reduce(f32[4]{0:T(128)S(1)} %dynamic-update-slice.1, f32[4]{0:T(128)S(1)} %dynamic-update-slice.4, f32[4]{0:T(128)S(1)} %dynamic-update-slice.5, f32[4]{0:T(128)S(1)} %dynamic-update-slice.7), channel_id=2, replica_groups=mesh['sp_0'=4,'sp_1'=4,'tp'=16] {'sp_0'}, use_global_device_ids=true, to_apply=%add.1 | all-reduce | flops 16 | bytes 128
  126.2 9.6 %all-gather.8 = f32[4,1,256]{2,1,0:T(1,128)S(1)} all-gather(f32[1,1,256]{2,1,0:T(1,128)S(1)} %bitcast.323), channel_id=9, replica_groups=mesh['sp_0'=4,'sp_1'=4,'tp'=16] {'sp_1'}, dimensions={0}, use_global_device_ids=true | all-gather | bytes 5120 | tf_op jit(solution)/shard_map/all_gather | solution.py:38
  135.9 7.0 %all_gather.81 = f32[4,1,256]{2,1,0:T(1,128)S(1)} all-gather(f32[1,1,256]{2,1,0:T(1,128)S(1)} %get-tuple-element.176), channel_id=1, replica_groups=mesh['sp_0'=4,'sp_1'=4,'tp'=16] {'sp_0'}, dimensions={0}, use_global_device_ids=true | all-gather | bytes 5120 | tf_op jit(solution)/shard_map/all_gather | solution.py:38
  145.2 2.6 multiply_reduce_fusion.1
  147.8 2.2 convolution_convert_fusion.1
  150.6 60.0 %reduce-scatter.3.cloned.1.call-done = bf16[32,2048]{1,0:T(8,128)(2,1)} async-done(((bf16[512,2048]{1,0:T(8,128)(2,1)}), bf16[32,2048]{1,0:T(8,128)(2,1)}) %reduce-scatter.3.cloned.1.call-update) | async-done | bytes 131088 | tf_op jit(solution)/shard_map/reduce_scatter | solution.py:233
  213.4 15.8 %all_to_all.10 = bf16[16,5,2048]{2,1,0:T(8,128)(2,1)S(1)} all-to-all(bf16[16,5,2048]{2,1,0:T(8,128)(2,1)S(1)} %reshape.898), channel_id=1, replica_groups=mesh['sp_0'=4,'sp_1'=4,'tp'=16] {'sp_0','sp_1'}, dimensions={0} | all-to-all | bytes 655360 | tf_op jit(solution)/shard_map/all_to_all | solution.py:260
  229.4 7.7 %collective-permute-done = bf16[80,2048]{1,0:T(8,128)(2,1)S(1)} collective-permute-done((bf16[80,2048]{1,0:T(8,128)(2,1)S(1)}, bf16[80,2048]{1,0:T(8,128)(2,1)S(1)}, u32[]{:S(2)}, u32[]{:S(2)}) %collective-permute-start) | collective-permute-done | bytes 327712 | tf_op jit(solution)/shard_map/ppermute | solution.py:20
  237.1 3.0 collective-permute-start.8
  240.0 4.8 %collective-permute-done.1 = bf16[80,2048]{1,0:T(8,128)(2,1)S(1)} collective-permute-done((bf16[80,2048]{1,0:T(8,128)(2,1)S(1)}, bf16[80,2048]{1,0:T(8,128)(2,1)S(1)}, u32[]{:S(2)}, u32[]{:S(2)}) %collective-permute-start.1) | collective-permute-done | bytes 327712 | tf_op jit(solution)/shard_map/ppermute | solution.py:20
  244.8 3.0 collective-permute-start.9
  247.7 4.7 %collective-permute-done.2 = bf16[80,2048]{1,0:T(8,128)(2,1)S(1)} collective-permute-done((bf16[80,2048]{1,0:T(8,128)(2,1)S(1)}, bf16[80,2048]{1,0:T(8,128)(2,1)S(1)}, u32[]{:S(2)}, u32[]{:S(2)}) %collective-permute-start.2) | collective-permute-done | bytes 327712 | tf_op jit(solution)/shard_map/ppermute | solution.py:20
  252.5 3.0 collective-permute-start.10
  255.4 4.7 %collective-permute-done.3 = bf16[80,2048]{1,0:T(8,128)(2,1)S(1)} collective-permute-done((bf16[80,2048]{1,0:T(8,128)(2,1)S(1)}, bf16[80,2048]{1,0:T(8,128)(2,1)S(1)}, u32[]{:S(2)}, u32[]{:S(2)}) %collective-permute-start.3) | collective-permute-done | bytes 327712 | tf_op jit(solution)/shard_map/ppermute | solution.py:20
  260.2 3.0 collective-permute-start.11
  263.2 4.7 %collective-permute-done.4 = bf16[80,2048]{1,0:T(8,128)(2,1)S(1)} collective-permute-done((bf16[80,2048]{1,0:T(8,128)(2,1)S(1)}, bf16[80,2048]{1,0:T(8,128)(2,1)S(1)}, u32[]{:S(2)}, u32[]{:S(2)}) %collective-permute-start.4) | collective-permute-done | bytes 327712 | tf_op jit(solution)/shard_map/ppermute | solution.py:20
  268.7 2.9 collective-permute-start.12
  271.6 4.0 collective-permute-done.5
  276.2 3.2 collective-permute-start.13
  279.4 4.0 collective-permute-done.6
  284.3 3.1 collective-permute-start.14
  287.4 4.0 collective-permute-done.7
  304.2 4.0 copy-done.14
  308.1 2.6 fusion.52
  310.8 10.9 %convolution_convert_fusion = bf16[1280,2048]{1,0:T(8,128)(2,1)} fusion(bf16[1,256,2048]{2,1,0:T(8,128)(2,1)S(1)} %copy-done, f32[1280,256]{1,0:T(8,128)} %fusion.52, bf16[1,2048,256]{2,1,0:T(8,128)(2,1)} %param.30, bf16[2560,2048]{1,0:T(8,128)(2,1)} %copy-done.14, s32[]{:T(128)S(6)} %select_n.533), kind=kOutput, calls=%fused_computation.75 | convolution fusion | flops 2688942080 | bytes 13893636 | tf_op jit(solution)/shard_map/dot_general | solution.py:268
  322.4 61.4 %reduce-scatter.5.cloned.1.call-done = bf16[80,2048]{1,0:T(8,128)(2,1)} async-done(((bf16[1280,2048]{1,0:T(8,128)(2,1)}), bf16[80,2048]{1,0:T(8,128)(2,1)}) %reduce-scatter.5.cloned.1.call-update) | async-done | bytes 327696 | tf_op jit(solution)/shard_map/reduce_scatter | solution.py:267
  385.7 7.3 %all-to-all-start.1 = ((bf16[16,5,2048]{2,1,0:T(8,128)(2,1)}), bf16[16,5,2048]{2,1,0:T(8,128)(2,1)S(1)}, u32[]{:S(2)}, u32[]{:S(2)}) async-start(bf16[16,5,2048]{2,1,0:T(8,128)(2,1)} %reshape.900), calls=%async_computation.3 | async-start | bytes 1048576 | tf_op jit(solution)/shard_map/all_to_all | solution.py:274
  393.0 8.8 %all-to-all-done.1 = bf16[16,5,2048]{2,1,0:T(8,128)(2,1)S(1)} async-done(((bf16[16,5,2048]{2,1,0:T(8,128)(2,1)}), bf16[16,5,2048]{2,1,0:T(8,128)(2,1)S(1)}, u32[]{:S(2)}, u32[]{:S(2)}) %all-to-all-start.1) | async-done | bytes 327712 | tf_op jit(solution)/shard_map/all_to_all | solution.py:274
  (222 shorter events, 74.1 us)
Async XLA Ops:
  6.5 304.2 %copy-start = (bf16[1,256,2048]{2,1,0:T(8,128)(2,1)S(1)}, bf16[1,256,2048]{2,1,0:T(8,128)(2,1)}, u32[]{:S(2)}) copy-start(bf16[1,256,2048]{2,1,0:T(8,128)(2,1)} %param.31) | copy-start | bytes 3145732
  6.5 40.4 %copy-start.21 = (u32[256]{0:T(256)S(1)}, u32[256]{0:T(256)}, u32[]{:S(2)}) copy-start(u32[256]{0:T(256)} %constant.152) | copy-start | bytes 3076
  6.5 70.9 %all-gather.14.cloned.1.call-start = ((), (), s32[]{:S(2)}) async-start(), calls=%async_computation.7 | async-start | bytes 1310720 | tf_op jit(solution)/shard_map/all_gather | solution.py:38
  10.0 69.4 %copy-start.20 = (u32[256]{0:T(256)S(1)}, u32[256]{0:T(256)}, u32[]{:S(2)}) copy-start(u32[256]{0:T(256)} %constant.157) | copy-start | bytes 3076
  10.0 132.8 %copy-start.13 = (s32[512]{0:T(512)S(1)}, s32[512]{0:T(512)}, u32[]{:S(2)}) copy-start(s32[512]{0:T(512)} %param.23) | copy-start | bytes 6148
  10.1 137.7 %copy-start.12 = (bf16[256,2048]{1,0:T(8,128)(2,1)S(1)}, bf16[256,2048]{1,0:T(8,128)(2,1)}, u32[]{:S(2)}) copy-start(bf16[256,2048]{1,0:T(8,128)(2,1)} %param.25) | copy-start | bytes 3145732
  10.1 137.7 %copy-start.18 = (f32[256]{0:T(256)S(1)}, f32[256]{0:T(256)}, u32[]{:S(2)}) copy-start(f32[256]{0:T(256)} %param.24) | copy-start | bytes 3076
  40.6 109.5 %copy-start.15 = (s32[32,2]{0,1:T(2,128)S(1)}, s32[32,2]{0,1:T(2,128)}, u32[]{:S(2)}) copy-start(s32[32,2]{0,1:T(2,128)} %param.27) | copy-start | bytes 772
  40.6 170.0 %copy-start.10 = (bf16[32,2048]{1,0:T(8,128)(2,1)S(1)}, bf16[32,2048]{1,0:T(8,128)(2,1)}, u32[]{:S(2)}) copy-start(bf16[32,2048]{1,0:T(8,128)(2,1)} %param.17) | copy-start | bytes 393220
  40.6 171.1 %copy-start.16 = (f32[2048]{0:T(1024)S(1)}, f32[2048]{0:T(1024)}, u32[]{:S(2)}) copy-start(f32[2048]{0:T(1024)} %param.26) | copy-start | bytes 24580
  41.4 103.9 %all-gather.12.cloned.1.call-start = ((), (), s32[]{:S(2)}) async-start(), calls=%async_computation.4 | async-start | bytes 1310720 | tf_op jit(solution)/shard_map/all_gather | solution.py:38
  79.4 131.2 %reduce-scatter.3.cloned.1.call-start = ((), (), s32[]{:S(2)}) async-start(), calls=%async_computation.5 | async-start | bytes 2228224 | tf_op jit(solution)/shard_map/reduce_scatter | solution.py:233
  150.0 233.8 %reduce-scatter.5.cloned.1.call-start = ((), (), s32[]{:S(2)}) async-start(), calls=%async_computation.6 | async-start | bytes 5570560 | tf_op jit(solution)/shard_map/reduce_scatter | solution.py:267
  229.3 7.7 %collective-permute-start = (bf16[80,2048]{1,0:T(8,128)(2,1)S(1)}, bf16[80,2048]{1,0:T(8,128)(2,1)S(1)}, u32[]{:S(2)}, u32[]{:S(2)}) collective-permute-start(bf16[80,2048]{1,0:T(8,128)(2,1)S(1)} %reshape.899), channel_id=1, source_target_pairs={{0,1},{1,2},{2,3},{3,4},{4,5},{5,6},{6,7},{7,8},{8,9},{9,10},{10,1... | collective-permute-start | bytes 983048 | tf_op jit(solution)/shard_map/ppermute | solution.py:20
  237.1 7.7 %collective-permute-start.1 = (bf16[80,2048]{1,0:T(8,128)(2,1)S(1)}, bf16[80,2048]{1,0:T(8,128)(2,1)S(1)}, u32[]{:S(2)}, u32[]{:S(2)}) collective-permute-start(bf16[80,2048]{1,0:T(8,128)(2,1)S(1)} %collective-permute-done), channel_id=1, source_target_pairs={{0,1},{1,2},{2,3},{3,4},{4,5},{5,6},{6,7},{7,8},{8,9},{9,10},{10,1... | collective-permute-start | bytes 983048 | tf_op jit(solution)/shard_map/ppermute | solution.py:20
  237.1 7.7 %collective-permute-start.8 = (bf16[80,2048]{1,0:T(8,128)(2,1)S(1)}, bf16[80,2048]{1,0:T(8,128)(2,1)S(1)}, u32[]{:S(2)}, u32[]{:S(2)}) collective-permute-start(bf16[80,2048]{1,0:T(8,128)(2,1)S(1)} %reshape.899), channel_id=1, source_target_pairs={{0,15},{1,0},{2,1},{3,2},{4,3},{5,4},{6,5},{7,6},{8,7},{9,8},{10,9... | collective-permute-start | bytes 983048 | tf_op jit(solution)/shard_map/ppermute | solution.py:22
  244.8 7.7 %collective-permute-start.2 = (bf16[80,2048]{1,0:T(8,128)(2,1)S(1)}, bf16[80,2048]{1,0:T(8,128)(2,1)S(1)}, u32[]{:S(2)}, u32[]{:S(2)}) collective-permute-start(bf16[80,2048]{1,0:T(8,128)(2,1)S(1)} %collective-permute-done.1), channel_id=1, source_target_pairs={{0,1},{1,2},{2,3},{3,4},{4,5},{5,6},{6,7},{7,8},{8,9},{9,10},{10,1... | collective-permute-start | bytes 983048 | tf_op jit(solution)/shard_map/ppermute | solution.py:20
  244.8 7.7 %collective-permute-start.9 = (bf16[80,2048]{1,0:T(8,128)(2,1)S(1)}, bf16[80,2048]{1,0:T(8,128)(2,1)S(1)}, u32[]{:S(2)}, u32[]{:S(2)}) collective-permute-start(bf16[80,2048]{1,0:T(8,128)(2,1)S(1)} %collective-permute-done.8), channel_id=1, source_target_pairs={{0,15},{1,0},{2,1},{3,2},{4,3},{5,4},{6,5},{7,6},{8,7},{9,8},{10,9... | collective-permute-start | bytes 983048 | tf_op jit(solution)/shard_map/ppermute | solution.py:22
  252.5 7.7 %collective-permute-start.3 = (bf16[80,2048]{1,0:T(8,128)(2,1)S(1)}, bf16[80,2048]{1,0:T(8,128)(2,1)S(1)}, u32[]{:S(2)}, u32[]{:S(2)}) collective-permute-start(bf16[80,2048]{1,0:T(8,128)(2,1)S(1)} %collective-permute-done.2), channel_id=1, source_target_pairs={{0,1},{1,2},{2,3},{3,4},{4,5},{5,6},{6,7},{7,8},{8,9},{9,10},{10,1... | collective-permute-start | bytes 983048 | tf_op jit(solution)/shard_map/ppermute | solution.py:20
  252.5 7.7 %collective-permute-start.10 = (bf16[80,2048]{1,0:T(8,128)(2,1)S(1)}, bf16[80,2048]{1,0:T(8,128)(2,1)S(1)}, u32[]{:S(2)}, u32[]{:S(2)}) collective-permute-start(bf16[80,2048]{1,0:T(8,128)(2,1)S(1)} %collective-permute-done.9), channel_id=1, source_target_pairs={{0,15},{1,0},{2,1},{3,2},{4,3},{5,4},{6,5},{7,6},{8,7},{9,8},{10,9... | collective-permute-start | bytes 983048 | tf_op jit(solution)/shard_map/ppermute | solution.py:22
  260.2 7.7 %collective-permute-start.4 = (bf16[80,2048]{1,0:T(8,128)(2,1)S(1)}, bf16[80,2048]{1,0:T(8,128)(2,1)S(1)}, u32[]{:S(2)}, u32[]{:S(2)}) collective-permute-start(bf16[80,2048]{1,0:T(8,128)(2,1)S(1)} %collective-permute-done.3), channel_id=1, source_target_pairs={{0,1},{1,2},{2,3},{3,4},{4,5},{5,6},{6,7},{7,8},{8,9},{9,10},{10,1... | collective-permute-start | bytes 983048 | tf_op jit(solution)/shard_map/ppermute | solution.py:20
  260.2 7.7 %collective-permute-start.11 = (bf16[80,2048]{1,0:T(8,128)(2,1)S(1)}, bf16[80,2048]{1,0:T(8,128)(2,1)S(1)}, u32[]{:S(2)}, u32[]{:S(2)}) collective-permute-start(bf16[80,2048]{1,0:T(8,128)(2,1)S(1)} %collective-permute-done.10), channel_id=1, source_target_pairs={{0,15},{1,0},{2,1},{3,2},{4,3},{5,4},{6,5},{7,6},{8,7},{9,8},{10,9... | collective-permute-start | bytes 983048 | tf_op jit(solution)/shard_map/ppermute | solution.py:22
  267.9 7.7 %collective-permute-start.5 = (bf16[80,2048]{1,0:T(8,128)(2,1)S(1)}, bf16[80,2048]{1,0:T(8,128)(2,1)S(1)}, u32[]{:S(2)}, u32[]{:S(2)}) collective-permute-start(bf16[80,2048]{1,0:T(8,128)(2,1)S(1)} %collective-permute-done.4), channel_id=1, source_target_pairs={{0,1},{1,2},{2,3},{3,4},{4,5},{5,6},{6,7},{7,8},{8,9},{9,10},{10,1... | collective-permute-start | bytes 983048 | tf_op jit(solution)/shard_map/ppermute | solution.py:20
  268.7 7.5 %collective-permute-start.12 = (bf16[80,2048]{1,0:T(8,128)(2,1)S(1)}, bf16[80,2048]{1,0:T(8,128)(2,1)}, u32[]{:S(2)}, u32[]{:S(2)}) collective-permute-start(bf16[80,2048]{1,0:T(8,128)(2,1)S(1)} %collective-permute-done.11), channel_id=1, source_target_pairs={{0,15},{1,0},{2,1},{3,2},{4,3},{5,4},{6,5},{7,6},{8,7},{9,8},{10,9... | collective-permute-start | bytes 983048 | tf_op jit(solution)/shard_map/ppermute | solution.py:22
  275.6 7.8 %collective-permute-start.6 = (bf16[80,2048]{1,0:T(8,128)(2,1)S(1)}, bf16[80,2048]{1,0:T(8,128)(2,1)}, u32[]{:S(2)}, u32[]{:S(2)}) collective-permute-start(bf16[80,2048]{1,0:T(8,128)(2,1)S(1)} %collective-permute-done.5), channel_id=1, source_target_pairs={{0,1},{1,2},{2,3},{3,4},{4,5},{5,6},{6,7},{7,8},{8,9},{9,10},{10,1... | collective-permute-start | bytes 983048 | tf_op jit(solution)/shard_map/ppermute | solution.py:20
  276.2 8.1 %collective-permute-start.13 = (bf16[80,2048]{1,0:T(8,128)(2,1)}, bf16[80,2048]{1,0:T(8,128)(2,1)}, u32[]{:S(2)}, u32[]{:S(2)}) collective-permute-start(bf16[80,2048]{1,0:T(8,128)(2,1)} %collective-permute-done.12), channel_id=1, source_target_pairs={{0,15},{1,0},{2,1},{3,2},{4,3},{5,4},{6,5},{7,6},{8,7},{9,8},{10,9... | collective-permute-start | bytes 983048 | tf_op jit(solution)/shard_map/ppermute | solution.py:22
  283.4 8.0 %collective-permute-start.7 = (bf16[80,2048]{1,0:T(8,128)(2,1)}, bf16[80,2048]{1,0:T(8,128)(2,1)}, u32[]{:S(2)}, u32[]{:S(2)}) collective-permute-start(bf16[80,2048]{1,0:T(8,128)(2,1)} %collective-permute-done.6), channel_id=1, source_target_pairs={{0,1},{1,2},{2,3},{3,4},{4,5},{5,6},{6,7},{7,8},{8,9},{9,10},{10,1... | collective-permute-start | bytes 983048 | tf_op jit(solution)/shard_map/ppermute | solution.py:20
  283.5 18.6 %copy-start.3 = (bf16[80,2048]{1,0:T(8,128)(2,1)S(1)}, bf16[80,2048]{1,0:T(8,128)(2,1)}, u32[]{:S(2)}) copy-start(bf16[80,2048]{1,0:T(8,128)(2,1)} %copy-done.2) | copy-start | bytes 983044
  283.5 24.7 %copy-start.19 = (bf16[1,2048,256]{2,1,0:T(8,128)(2,1)S(1)}, bf16[1,2048,256]{2,1,0:T(8,128)(2,1)}, u32[]{:S(2)}) copy-start(bf16[1,2048,256]{2,1,0:T(8,128)(2,1)} %param.29) | copy-start | bytes 3145732
  284.3 15.4 %collective-permute-start.14 = (bf16[80,2048]{1,0:T(8,128)(2,1)}, bf16[80,2048]{1,0:T(8,128)(2,1)S(1)}, u32[]{:S(2)}, u32[]{:S(2)}) collective-permute-start(bf16[80,2048]{1,0:T(8,128)(2,1)} %collective-permute-done.13), channel_id=1, source_target_pairs={{0,15},{1,0},{2,1},{3,2},{4,3},{5,4},{6,5},{7,6},{8,7},{9,8},{10,9... | collective-permute-start | bytes 983048 | tf_op jit(solution)/shard_map/ppermute | solution.py:22
  321.7 82.8 %copy-start.11 = (bf16[32,2048]{1,0:T(8,128)(2,1)S(1)}, bf16[32,2048]{1,0:T(8,128)(2,1)}, u32[]{:S(2)}) copy-start(bf16[32,2048]{1,0:T(8,128)(2,1)} %reduce-scatter.3.cloned.1.call-done) | copy-start | bytes 393220
  385.7 16.0 %all-to-all-start.1 = ((bf16[16,5,2048]{2,1,0:T(8,128)(2,1)}), bf16[16,5,2048]{2,1,0:T(8,128)(2,1)S(1)}, u32[]{:S(2)}, u32[]{:S(2)}) async-start(bf16[16,5,2048]{2,1,0:T(8,128)(2,1)} %reshape.900), calls=%async_computation.3 | async-start | bytes 1048576 | tf_op jit(solution)/shard_map/all_to_all | solution.py:274
  (10 other events, 107.2 us)
Sparse Core Ops, SparseCore 0:
  41.5 28.4 all-gather.13
  79.5 28.0 all-gather.11
  150.1 60.4 reduce-scatter.2
  321.9 61.8 reduce-scatter.4
